TPU v7x, 32 devices: a whole 2x2x4 slice. The times are simulated.
32 devices in a mesh: sp: 16 (over z, y, x), tp: 2 (over core).
Axes of the slice: x: 2, y: 2, z: 4, core: 2. Of those that a mesh axis runs over, the one named last changes fastest.
Arguments:
- prompt: bfloat16 [1, 8192, 2048], P(None, 'sp', 'tp'), may hold values from -6 to 6
- new_token: bfloat16 [1, 2048], P(None, 'tp'), may hold values from -6 to 6
- w_query: bfloat16 [2048, 2048], P(None, 'tp'), may hold values from -0.125 to 0.125
- w_key: bfloat16 [2048, 2048], P(None, 'tp'), may hold values from -0.125 to 0.125
- w_value: bfloat16 [2048, 2048], P(None, 'tp'), may hold values from -0.125 to 0.125
- decay_rate: float32 [16], P('tp'), may hold values from 1e-05 to 0.06
- norm_gain: float32 [2048], P('tp'), may hold values from 0.1 to 1.9
Outputs:
- mixed: bfloat16 [1, 8192, 2048], P(None, 'sp', 'tp')
- cache: bfloat16 [1, 16, 128, 128], P(None, 'tp', 'sp')
- new_read: bfloat16 [1, 2048], P(None, 'tp')
All inputs are finite; a program needn't handle non-finite values.
Results may differ from a plain program's by a relative error of at most 0.0083.
Values may be sent and summed in bfloat16 or wider, within the bound.
A program may use at most 64 MiB of HBM per device.

v0:
```python
import jax
import jax.numpy as jnp
from jax import lax
from jax.sharding import PartitionSpec as P

HEAD = 128
rope_base = 10000.0
norm_floor = 1e-05


def rotate(tensor, positions):
    head_width = tensor.shape[-1]
    inverse = rope_base ** (-jnp.arange(0, head_width, 2, dtype=jnp.float32) / head_width)
    angles = positions.astype(jnp.float32)[:, None] * inverse[None, :]
    cosine = jnp.cos(angles)[:, None, :]
    sine_part = jnp.sin(angles)[:, None, :]
    first_half = tensor[..., : head_width // 2]
    second_half = tensor[..., head_width // 2 :]
    return jnp.concatenate(
        [
            first_half * cosine - second_half * sine_part,
            first_half * sine_part + second_half * cosine,
        ],
        axis=-1,
    )


def head_norm(output, gain):
    center = jnp.mean(output, axis=-1, keepdims=True)
    spread = jnp.mean(jnp.square(output - center), axis=-1, keepdims=True)
    return (output - center) * lax.rsqrt(spread + norm_floor) * gain


def decay_tables(log_gamma, block_size):
    offsets = jnp.arange(block_size, dtype=jnp.float32)
    gap_table = offsets[:, None] - offsets[None, :]
    within = jnp.where(
        gap_table[None] >= 0,
        jnp.exp(jnp.maximum(gap_table, 0.0)[None] * log_gamma[:, None, None]),
        0.0,
    )
    query_decay = jnp.exp((offsets[:, None] + 1.0) * log_gamma[None, :])
    key_decay = jnp.exp((block_size - 1.0 - offsets[:, None]) * log_gamma[None, :])
    return (within, query_decay, key_decay)


def per_device(prompt, new_token, w_query, w_key, w_value, decay_rate, norm_gain):
    sequences, block_size, feature_part = prompt.shape
    head_count = w_query.shape[1] // HEAD
    members = lax.axis_size("sp")
    device_rank = lax.axis_index("sp")
    prompt_rows = sequences * block_size
    token_rows = jnp.concatenate([prompt.reshape(prompt_rows, feature_part), new_token], axis=0)
    weight_list = (w_query, w_key, w_value)
    shard_piece = lax.all_gather(token_rows, "tp", axis=1, tiled=True)
    projected = tuple(
        (jnp.dot(shard_piece, weight, preferred_element_type=jnp.float32) for weight in weight_list)
    )
    full_shape = (sequences, block_size, head_count, HEAD)
    queries, key_rows, values = [
        tensor[:prompt_rows].astype(jnp.bfloat16).reshape(full_shape) for tensor in projected
    ]
    token_query, token_key, token_value = [
        tensor[prompt_rows:].astype(jnp.bfloat16).reshape(sequences, 1, head_count, HEAD)
        for tensor in projected
    ]
    positions = device_rank * block_size + jnp.arange(block_size, dtype=jnp.int32)
    scaled = (rotate(queries.astype(jnp.float32), positions) * HEAD ** (-0.5)).astype(jnp.bfloat16)
    turned = rotate(key_rows.astype(jnp.float32), positions).astype(jnp.bfloat16)
    log_gamma = -decay_rate
    within, query_decay, key_decay = decay_tables(log_gamma, block_size)
    weighted = (turned.astype(jnp.float32) * key_decay[None, :, :, None]).astype(jnp.bfloat16)
    local_state = jnp.einsum(
        "smhd,smhe->shde", weighted, values, preferred_element_type=jnp.float32
    )
    pieces = lax.all_to_all(local_state[None], "sp", split_axis=3, concat_axis=0, tiled=True)
    source_index = jnp.arange(members, dtype=jnp.float32)
    gap_table = source_index[:, None] - 1.0 - source_index[None, :]
    weights = jnp.where(
        gap_table[None] >= 0,
        jnp.exp(jnp.maximum(gap_table, 0.0)[None] * block_size * log_gamma[:, None, None]),
        0.0,
    )
    prefix = jnp.einsum("hji,ishre->jshre", weights, pieces, precision=lax.Precision.HIGHEST)
    tail_all = jnp.exp((members - 1.0 - source_index)[None, :] * block_size * log_gamma[:, None])
    final_rows = jnp.einsum("hi,ishre->shre", tail_all, pieces, precision=lax.Precision.HIGHEST)
    incoming = lax.all_to_all(
        prefix.astype(jnp.bfloat16), "sp", split_axis=0, concat_axis=3, tiled=True
    ).astype(prefix.dtype)[0]
    scores = (
        jnp.einsum("snhd,smhd->shnm", scaled, turned, preferred_element_type=jnp.float32)
        * within[None]
    )
    inner_part = jnp.einsum(
        "shnm,smhe->snhe", scores.astype(jnp.bfloat16), values, preferred_element_type=jnp.float32
    )
    carried = (
        jnp.einsum(
            "snhd,shde->snhe",
            scaled,
            incoming.astype(jnp.bfloat16),
            preferred_element_type=jnp.float32,
        )
        * query_decay[None, :, :, None]
    )
    gain = norm_gain.reshape(head_count, HEAD)
    mixed = (
        head_norm(inner_part + carried, gain)
        .astype(jnp.bfloat16)
        .reshape(sequences, block_size, head_count * HEAD)
    )
    cache = final_rows.astype(jnp.bfloat16)
    token_positions = jnp.full((1,), block_size * members, jnp.int32)
    token_scaled = (
        rotate(token_query.astype(jnp.float32), token_positions) * HEAD ** (-0.5)
    ).astype(jnp.bfloat16)[:, 0]
    token_turned = rotate(token_key.astype(jnp.float32), token_positions).astype(jnp.bfloat16)[:, 0]
    row_count = final_rows.shape[2]
    query_rows = lax.dynamic_slice_in_dim(
        token_scaled, device_rank * row_count, row_count, 2
    ).astype(jnp.float32)
    partial_value = jnp.einsum(
        "shr,shre->she", query_rows, final_rows, precision=lax.Precision.HIGHEST
    )
    read_sum = lax.psum(partial_value, "sp")
    own_score = jnp.sum(
        token_scaled.astype(jnp.float32) * token_turned.astype(jnp.float32), axis=-1, keepdims=True
    )
    read_out = jnp.exp(log_gamma)[None, :, None] * read_sum + own_score * token_value[:, 0].astype(
        jnp.float32
    )
    new_read = head_norm(read_out, gain).astype(jnp.bfloat16).reshape(sequences, head_count * HEAD)
    return (mixed, cache, new_read)


def solution(mesh):
    in_specs = (
        P(None, "sp", "tp"),
        P(None, "tp"),
        P(None, "tp"),
        P(None, "tp"),
        P(None, "tp"),
        P("tp"),
        P("tp"),
    )
    out_specs = (P(None, "sp", "tp"), P(None, "tp", "sp", None), P(None, "tp"))
    return jax.shard_map(
        per_device, mesh=mesh, in_specs=in_specs, out_specs=out_specs, check_vma=False
    )
```

profile of v0, /device:TPU:0, one launch (start us, length us, event | category | flops | bytes accessed | tf_op | source)
XLA Modules:
  0.0 131.3 jit_solution(5846563984525811698)
XLA Ops:
  7.2 0.0 all-gather.2.cloned.1.call-start
  7.2 0.0 copy-start.8
  7.2 2.3 %pad_maximum_fusion = bf16[513,1024]{1,0:T(8,128)(2,1)} fusion(bf16[1,1024]{1,0:T(2,128)(2,1)} %param.8, bf16[512,1024]{1,0:T(8,128)(2,1)} %bitcast.117), kind=kLoop, calls=%fused_computation.26 | loop fusion | flops 2101248 | bytes 2101248 | tf_op jit(solution)/shard_map/concatenate | solution.py:53
  9.6 0.0 all-gather.2.cloned.1.call-update
  9.6 0.1 multiply_sine_fusion.1
  9.7 0.3 fusion.16
  10.0 1.2 fusion.15
  11.1 0.0 copy-done.8
  11.1 0.1 fusion.34
  11.2 0.1 multiply_exponential_fusion.2
  11.3 0.1 maximum_multiply_fusion.1
  11.3 0.1 multiply_exponential_fusion.1
  11.4 1.0 multiply_cosine_fusion
  12.4 10.7 %all-gather.2.cloned.1.call-done = bf16[513,2048]{1,0:T(8,128)(2,1)} async-done(((bf16[513,1024]{1,0:T(8,128)(2,1)}), bf16[513,2048]{1,0:T(8,128)(2,1)}) %all-gather.2.cloned.1.call-update) | async-done | bytes 2101264 | tf_op jit(solution)/shard_map/all_gather | solution.py:55
  23.1 0.0 copy-start.5
  23.1 5.3 %convolution_convert_fusion = bf16[513,1024]{1,0:T(8,128)(2,1)S(1)} fusion(bf16[513,2048]{1,0:T(8,128)(2,1)} %all-gather.2.cloned.1.call-done, bf16[2048,1024]{1,0:T(8,128)(2,1)} %param.10), kind=kOutput, calls=%fused_computation.20 | convolution fusion | flops 2152203264 | bytes 7346176 | tf_op jit(solution)/shard_map/dot_general | solution.py:57
  28.4 0.0 copy-start.7
  28.5 0.2 convert_bitcast_fusion
  28.7 0.0 copy-done.5
  28.7 1.3 %copy-done.7 = bf16[513,2048]{1,0:T(8,128)(2,1)S(1)} copy-done((bf16[513,2048]{1,0:T(8,128)(2,1)S(1)}, bf16[513,2048]{1,0:T(8,128)(2,1)}, u32[]{:S(2)}) %copy-start.7) | copy-done | bytes 2101272
  30.0 2.4 %convolution_convert_fusion.1 = bf16[513,1024]{1,0:T(8,128)(2,1)S(1)} fusion(bf16[513,2048]{1,0:T(8,128)(2,1)S(1)} %copy-done.7, bf16[2048,1024]{1,0:T(8,128)(2,1)S(1)} %copy-done.5), kind=kOutput, calls=%fused_computation.21 | convolution fusion | flops 2152203264 | bytes 7346176 | tf_op jit(solution)/shard_map/dot_general | solution.py:57
  32.5 0.2 convert_bitcast_fusion.1
  32.7 0.5 copy.71
  33.2 0.5 copy.70
  33.7 1.3 %fusion.49 = (f32[1,512,8,64]{3,2,1,0:T(8,128)S(1)}, f32[1,512,8,64]{3,2,1,0:T(8,128)S(1)}, f32[1,512,8,64]{3,2,1,0:T(8,128)S(1)}, f32[1,512,8,64]{3,2,1,0:T(8,128)S(1)}) fusion(f32[1,512,8,128]{3,2,1,0:T(8,128)S(1)} %bitcast.112, f32[1,512,8,128]{3,2,1,0:T(8,128)S(1)} %bitcast.113), kind=kLoop, calls=%fused_computation.104 | loop fusion | bytes 8388608 | tf_op jit(solution)/shard_map/slice | solution.py:17
  35.0 0.0 copy-start.6
  35.0 2.8 %fusion.10 = (bf16[512,8,64]{2,0,1:T(8,128)(2,1)S(1)}, bf16[512,8,64]{2,0,1:T(8,128)(2,1)S(1)}, f32[512,8,64]{2,0,1:T(8,128)S(1)}, f32[512,8,64]{2,0,1:T(8,128)}) fusion(f32[1,512,8,64]{3,2,1,0:T(8,128)S(1)} %get-tuple-element.22, f32[1,512,8,64]{3,2,1,0:T(8,128)S(1)} %get-tuple-element.21, f32[512,64]{1,0:T(8,128)S(1)} %get-tuple-element.32, ...), kind=kLoop, calls=%fused_computation.27 | loop fusion | flops 3670016 | bytes 7602176 | tf_op jit(solution)/shard_map/concatenate | solution.py:19
  37.9 0.0 copy-done.6
  37.9 0.0 copy-start.1
  37.9 0.0 copy-start.2
  37.9 2.4 %convolution_convert_fusion.2 = bf16[513,1024]{1,0:T(8,128)(2,1)S(1)} fusion(bf16[513,2048]{1,0:T(8,128)(2,1)S(1)} %copy-done.7, bf16[2048,1024]{1,0:T(8,128)(2,1)S(1)} %copy-done.6), kind=kOutput, calls=%fused_computation.22 | convolution fusion | flops 2152203264 | bytes 7346176 | tf_op jit(solution)/shard_map/dot_general | solution.py:57
  40.3 0.0 copy-start.4
  40.3 0.0 copy-done.1
  40.3 0.0 copy-done.2
  40.3 2.6 %convolution_bitcast_fusion = f32[1,1,8,128,128]{4,3,2,1,0:T(8,128)S(1)} fusion(f32[512,8]{0,1:T(8,128)S(1)} %get-tuple-element.37, bf16[512,8,64]{2,0,1:T(8,128)(2,1)S(1)} %get-tuple-element.18, bf16[512,8,64]{2,0,1:T(8,128)(2,1)S(1)} %get-tuple-element.17, bf16[513,1024]{1,0:T(8,128)(2,1)S(1)} %convolution_convert_fusion.2), kind=kOutput, calls=%fused_computation.23 | convolution fusion | flops 137363456 | bytes 3686400 | tf_op jit(solution)/shard_map/smhd,smhe->shde/dot_general | solution.py:73
  42.9 0.0 copy-done.4
  43.0 1.1 copy.49
  44.1 6.8 %all-to-all-start = ((f32[1,1,8,128,128]{4,2,1,0,3:T(8,128)}), f32[1,1,8,128,128]{4,2,1,0,3:T(8,128)S(1)}, u32[]{:S(2)}, u32[]{:S(2)}) async-start(f32[1,1,8,128,128]{4,2,1,0,3:T(8,128)} %copy.49), calls=%async_computation | async-start | bytes 1048576 | tf_op jit(solution)/shard_map/all_to_all | solution.py:76
  50.9 0.1 fusion.40
  51.0 0.1 fusion.35
  51.0 0.1 dynamic-slice_bitcast_fusion
  51.1 0.2 multiply_reduce_fusion.2
  51.3 3.2 %fusion.7 = bf16[512,8,128]{2,0,1:T(8,128)(2,1)} fusion(f32[512,8,64]{2,0,1:T(8,128)S(1)} %get-tuple-element.25, f32[512,8,64]{2,0,1:T(8,128)} %get-tuple-element.26), kind=kLoop, calls=%fused_computation.8 | loop fusion | flops 1572864 | bytes 3145728 | tf_op jit(solution)/shard_map/convert_element_type | solution.py:68
  54.5 0.7 slice_convert_fusion
  55.2 7.4 %fusion = f32[8,128,512]{2,1,0:T(8,128)} fusion(f32[8]{0:T(128)S(1)} %get-tuple-element.36, f32[512,512]{1,0:T(8,128)} %fusion.15, pred[512,512]{1,0:T(8,128)(4,1)S(1)} %fusion.16, bf16[512,8,128]{2,0,1:T(8,128)(2,1)} %fusion.7, bf16[512,8,64]{2,0,1:T(8,128)(2,1)} %copy-done.2, bf16[512,8,64]{2,0,1:T(8,128)(2,1)} %copy-done.1, bf16[513,1024]{1,0:T(8,128)(2,1)} %copy-done.4), kind=kOutput, calls=%fused_computation.1 | convolution fusion | flops 1084227584 | bytes 7602208 | tf_op jit(solution)/shard_map/shnm,smhe->snhe/dot_general | solution.py:94
  62.6 3.8 %all-to-all-done = f32[1,1,8,128,128]{4,2,1,0,3:T(8,128)S(1)} async-done(((f32[1,1,8,128,128]{4,2,1,0,3:T(8,128)}), f32[1,1,8,128,128]{4,2,1,0,3:T(8,128)S(1)}, u32[]{:S(2)}, u32[]{:S(2)}) %all-to-all-start) | async-done | bytes 524320 | tf_op jit(solution)/shard_map/all_to_all | solution.py:76
  66.4 0.7 fusion.19
  67.1 0.9 fusion.9
  68.0 0.8 copy.52
  68.7 0.1 fusion.38
  68.9 39.2 %psum.7 = f32[1,8,128]{2,1,0:T(8,128)S(1)} all-reduce(f32[1,8,128]{2,1,0:T(8,128)S(1)} %bitcast.127), channel_id=1, replica_groups=mesh['sp'=16,'tp'=2] {'sp'}, use_global_device_ids=true, to_apply=%region_2.3 | all-reduce | flops 1024 | bytes 8192 | tf_op jit(solution)/shard_map/psum | solution.py:125
  108.1 0.2 fusion.48
  108.3 3.5 %all-to-all-start.1 = ((bf16[16,1,8,8,128]{4,3,2,1,0:T(8,128)(2,1)}), bf16[16,1,8,8,128]{4,3,2,1,0:T(8,128)(2,1)S(1)}, u32[]{:S(2)}, u32[]{:S(2)}) async-start(bf16[16,1,8,8,128]{4,3,2,1,0:T(8,128)(2,1)} %copy.52), calls=%async_computation.1 | async-start | bytes 524288 | tf_op jit(solution)/shard_map/all_to_all | solution.py:87
  111.8 0.2 multiply_reduce_fusion.1
  112.0 0.0 copy-done.3
  112.0 0.1 fusion.42
  112.1 0.6 copy.114
  112.7 0.6 convert_bitcast_fusion.2
  113.3 7.0 %all-to-all-done.1 = bf16[16,1,8,8,128]{4,3,2,1,0:T(8,128)(2,1)S(1)} async-done(((bf16[16,1,8,8,128]{4,3,2,1,0:T(8,128)(2,1)}), bf16[16,1,8,8,128]{4,3,2,1,0:T(8,128)(2,1)S(1)}, u32[]{:S(2)}, u32[]{:S(2)}) %all-to-all-start.1) | async-done | bytes 262176 | tf_op jit(solution)/shard_map/all_to_all | solution.py:87
  120.3 0.0 copy-done
  120.3 2.1 %fusion.51 = (f32[512,8]{0,1:T(8,128)S(1)}, f32[1,512,8,128]{1,3,2,0:T(8,128)S(1)}) fusion(f32[512,8]{0,1:T(8,128)S(1)} %get-tuple-element.38, bf16[512,8,128]{2,0,1:T(8,128)(2,1)S(1)} %copy-done, bf16[16,1,8,8,128]{4,3,2,1,0:T(8,128)(2,1)S(1)} %all-to-all-done.1, f32[8,128,512]{2,1,0:T(8,128)} %fusion), kind=kOutput, calls=%fused_computation.106 | convolution fusion | flops 135786496 | bytes 5537792 | tf_op jit(solution)/shard_map/snhd,shde->snhe/dot_general | solution.py:98
  122.4 0.3 multiply_reduce_fusion
  122.8 0.4 multiply_convert_fusion.2
  123.1 1.3 %copy.55 = bf16[1,512,1024]{2,1,0:T(8,128)(2,1)} copy(bf16[1,512,1024]{1,2,0:T(8,128)(2,1)S(1)} %bitcast.116) | data formatting | bytes 2097152
  (14 shorter events, 0.1 us)
Async XLA Ops:
  7.2 15.9 %all-gather.2.cloned.1.call-start = ((), (), s32[]{:S(2)}) async-start(), calls=%async_computation.2 | async-start | bytes 3194880 | tf_op jit(solution)/shard_map/all_gather | solution.py:55
  7.2 3.9 %copy-start.8 = (f32[8]{0:T(128)S(1)}, f32[8]{0:T(128)}, u32[]{:S(2)}) copy-start(f32[8]{0:T(128)} %param.12) | copy-start | bytes 100
  23.1 5.6 %copy-start.5 = (bf16[2048,1024]{1,0:T(8,128)(2,1)S(1)}, bf16[2048,1024]{1,0:T(8,128)(2,1)}, u32[]{:S(2)}) copy-start(bf16[2048,1024]{1,0:T(8,128)(2,1)} %param.9) | copy-start | bytes 12582916
  28.4 1.6 %copy-start.7 = (bf16[513,2048]{1,0:T(8,128)(2,1)S(1)}, bf16[513,2048]{1,0:T(8,128)(2,1)}, u32[]{:S(2)}) copy-start(bf16[513,2048]{1,0:T(8,128)(2,1)} %all-gather.2.cloned.1.call-done) | copy-start | bytes 6303748
  35.0 2.8 %copy-start.6 = (bf16[2048,1024]{1,0:T(8,128)(2,1)S(1)}, bf16[2048,1024]{1,0:T(8,128)(2,1)}, u32[]{:S(2)}) copy-start(bf16[2048,1024]{1,0:T(8,128)(2,1)} %param.11) | copy-start | bytes 12582916
  37.9 2.4 %copy-start.1 = (bf16[512,8,64]{2,0,1:T(8,128)(2,1)}, bf16[512,8,64]{2,0,1:T(8,128)(2,1)S(1)}, u32[]{:S(2)}) copy-start(bf16[512,8,64]{2,0,1:T(8,128)(2,1)S(1)} %get-tuple-element.17) | copy-start | bytes 1572868
  37.9 2.4 %copy-start.2 = (bf16[512,8,64]{2,0,1:T(8,128)(2,1)}, bf16[512,8,64]{2,0,1:T(8,128)(2,1)S(1)}, u32[]{:S(2)}) copy-start(bf16[512,8,64]{2,0,1:T(8,128)(2,1)S(1)} %get-tuple-element.18) | copy-start | bytes 1572868
  40.3 2.7 %copy-start.4 = (bf16[513,1024]{1,0:T(8,128)(2,1)}, bf16[513,1024]{1,0:T(8,128)(2,1)S(1)}, u32[]{:S(2)}) copy-start(bf16[513,1024]{1,0:T(8,128)(2,1)S(1)} %convolution_convert_fusion.2) | copy-start | bytes 3151876
  44.1 22.3 %all-to-all-start = ((f32[1,1,8,128,128]{4,2,1,0,3:T(8,128)}), f32[1,1,8,128,128]{4,2,1,0,3:T(8,128)S(1)}, u32[]{:S(2)}, u32[]{:S(2)}) async-start(f32[1,1,8,128,128]{4,2,1,0,3:T(8,128)} %copy.49), calls=%async_computation | async-start | bytes 1048576 | tf_op jit(solution)/shard_map/all_to_all | solution.py:76
  62.6 49.4 %copy-start.3 = (f32[1024]{0:T(1024)S(1)}, f32[1024]{0:T(1024)}, u32[]{:S(2)}) copy-start(f32[1024]{0:T(1024)} %param.13) | copy-start | bytes 12292
  62.6 57.7 %copy-start = (bf16[512,8,128]{2,0,1:T(8,128)(2,1)S(1)}, bf16[512,8,128]{2,0,1:T(8,128)(2,1)}, u32[]{:S(2)}) copy-start(bf16[512,8,128]{2,0,1:T(8,128)(2,1)} %fusion.7) | copy-start | bytes 3145732
  108.3 12.0 %all-to-all-start.1 = ((bf16[16,1,8,8,128]{4,3,2,1,0:T(8,128)(2,1)}), bf16[16,1,8,8,128]{4,3,2,1,0:T(8,128)(2,1)S(1)}, u32[]{:S(2)}, u32[]{:S(2)}) async-start(bf16[16,1,8,8,128]{4,3,2,1,0:T(8,128)(2,1)} %copy.52), calls=%async_computation.1 | async-start | bytes 524288 | tf_op jit(solution)/shard_map/all_to_all | solution.py:87
Sparse Core Ops, SparseCore 0:
  9.7 13.3 all-gather.1
where the time goes:
time: 132 us; the launch traced here: 131 us
  blocking collectives  39.2 us (30%)
  matrix products  24.1 us (18%)
  waiting for transfers between devices  21.4 us (16%)
  other arithmetic  14.4 us (11%)
  between operations  14.3 us (11%)
  starting transfers between devices  10.4 us (8%)
  local copies, waits for them, and re-layouts  7.52 us (6%)
    psum x1, blocking collectives, per_device(): read_sum = lax.psum(partial_value, 'sp')  39.2 us
    all_gather x1, waiting for transfers between devices, per_device(): shard_piece = lax.all_gather(token_rows, 'tp', axis=1, tiled=True)  10.7 us
    dot_general x3, matrix products, per_device(): jnp.dot(shard_piece, weight, preferred_element_type=jnp.float32)  10.2 us
    dot_general x1, matrix products, per_device(): jnp.einsum('shnm,smhe->snhe', scores.astype(jnp.bfloat16), values, prefer...  7.39 us
    all_to_all x1, waiting for transfers between devices, per_device(): lax.all_to_all(prefix.astype(jnp.bfloat16), 'sp', split_axis=0, concat_ax...  6.98 us
    all_to_all x1, starting transfers between devices, per_device(): lax.all_to_all(local_state[None], 'sp', split_axis=3, concat_axis=0, tile...  6.79 us
    unnamed x22, local copies, waits for them, and re-layouts  4.22 us
    all_to_all x1, waiting for transfers between devices, per_device(): lax.all_to_all(local_state[None], 'sp', split_axis=3, concat_axis=0, tile...  3.77 us
  transfers between devices with their start and end apart: 3, of which 3 were waited for; matrix products, arithmetic and copies ran while one was open for 12% of the time, Pallas kernels for 0%

commit v1 on v0

--- a/solution.py
+++ b/solution.py
@@ -84,8 +84,14 @@
     prefix = jnp.einsum("hji,ishre->jshre", weights, pieces, precision=lax.Precision.HIGHEST)
     tail_all = jnp.exp((members - 1.0 - source_index)[None, :] * block_size * log_gamma[:, None])
     final_rows = jnp.einsum("hi,ishre->shre", tail_all, pieces, precision=lax.Precision.HIGHEST)
-    incoming = lax.all_to_all(
-        prefix.astype(jnp.bfloat16), "sp", split_axis=0, concat_axis=3, tiled=True
+    incoming = jnp.concatenate(
+        lax.all_to_all(
+            jnp.stack(jnp.split(prefix.astype(jnp.bfloat16), lax.axis_size("sp"), axis=0)),
+            "sp",
+            0,
+            0,
+        ),
+        axis=3,
     ).astype(prefix.dtype)[0]
     scores = (
         jnp.einsum("snhd,smhd->shnm", scaled, turned, preferred_element_type=jnp.float32)

time: 132 us -> 141 us (1.068)
  local copies, waits for them, and re-layouts: 7.52 us -> 16.9 us
    unnamed x22 -> x37, local copies, waits for them, and re-layouts: 4.22 us -> 13.3 us
  transfers between devices with their start and end apart: 3 -> 3, of which waited for: 3 -> 3; matrix products, arithmetic and copies ran while one was open for 12% -> 11% of each run, Pallas kernels for 0% -> 0%
where the time goes in v1:
time: 141 us
  blocking collectives  39.2 us (28%)
  matrix products  24.1 us (17%)
  waiting for transfers between devices  21.4 us (15%)
  local copies, waits for them, and re-layouts  16.9 us (12%)
  other arithmetic  14.4 us (10%)
  between operations  14.3 us (10%)
  starting transfers between devices  10.4 us (7%)
    psum x1, blocking collectives, per_device(): read_sum = lax.psum(partial_value, 'sp')  39.2 us
    unnamed x37, local copies, waits for them, and re-layouts  13.3 us
    all_gather x1, waiting for transfers between devices, per_device(): shard_piece = lax.all_gather(token_rows, 'tp', axis=1, tiled=True)  10.6 us
    dot_general x3, matrix products, per_device(): jnp.dot(shard_piece, weight, preferred_element_type=jnp.float32)  10.2 us
    dot_general x1, matrix products, per_device(): jnp.einsum('shnm,smhe->snhe', scores.astype(jnp.bfloat16), values, prefer...  7.4 us
    all_to_all x1, waiting for transfers between devices, per_device(): lax.all_to_all(jnp.stack(jnp.split(prefix.astype(jnp.bfloat16), lax.axis_...  6.98 us
    all_to_all x1, starting transfers between devices, per_device(): lax.all_to_all(local_state[None], 'sp', split_axis=3, concat_axis=0, tile...  6.8 us
    all_to_all x1, waiting for transfers between devices, per_device(): lax.all_to_all(local_state[None], 'sp', split_axis=3, concat_axis=0, tile...  3.76 us
  transfers between devices with their start and end apart: 3, of which 3 were waited for; matrix products, arithmetic and copies ran while one was open for 11% of the time, Pallas kernels for 0%

profile of v1, /device:TPU:0, one launch (start us, length us, event | category | flops | bytes accessed | tf_op | source)
XLA Modules:
  0.0 140.7 jit_solution(18393202517669038599)
XLA Ops:
  7.2 0.0 all-gather.2.cloned.1.call-start
  7.2 2.3 %pad_maximum_fusion = bf16[513,1024]{1,0:T(8,128)(2,1)} fusion(bf16[1,1024]{1,0:T(2,128)(2,1)} %param.8, bf16[512,1024]{1,0:T(8,128)(2,1)} %bitcast.149), kind=kLoop, calls=%fused_computation.26 | loop fusion | flops 2101248 | bytes 2101248 | tf_op jit(solution)/shard_map/concatenate | solution.py:53
  9.6 0.1 multiply_sine_fusion.1
  9.7 0.3 fusion.16
  9.9 1.2 fusion.15
  11.1 0.1 fusion.34
  11.2 0.1 multiply_exponential_fusion.2
  11.3 0.1 maximum_multiply_fusion.1
  11.3 0.1 multiply_exponential_fusion.1
  11.4 1.0 multiply_cosine_fusion
  12.4 10.6 %all-gather.2.cloned.1.call-done = bf16[513,2048]{1,0:T(8,128)(2,1)} async-done(((bf16[513,1024]{1,0:T(8,128)(2,1)}), bf16[513,2048]{1,0:T(8,128)(2,1)}) %all-gather.2.cloned.1.call-update) | async-done | bytes 2101264 | tf_op jit(solution)/shard_map/all_gather | solution.py:55
  23.1 5.3 %convolution_convert_fusion = bf16[513,1024]{1,0:T(8,128)(2,1)S(1)} fusion(bf16[513,2048]{1,0:T(8,128)(2,1)} %all-gather.2.cloned.1.call-done, bf16[2048,1024]{1,0:T(8,128)(2,1)} %param.10), kind=kOutput, calls=%fused_computation.20 | convolution fusion | flops 2152203264 | bytes 7346176 | tf_op jit(solution)/shard_map/dot_general | solution.py:57
  28.4 0.2 convert_bitcast_fusion
  28.7 1.3 copy-done.7
  30.0 2.4 %convolution_convert_fusion.1 = bf16[513,1024]{1,0:T(8,128)(2,1)S(1)} fusion(bf16[513,2048]{1,0:T(8,128)(2,1)S(1)} %copy-done.7, bf16[2048,1024]{1,0:T(8,128)(2,1)S(1)} %copy-done.5), kind=kOutput, calls=%fused_computation.21 | convolution fusion | flops 2152203264 | bytes 7346176 | tf_op jit(solution)/shard_map/dot_general | solution.py:57
  32.4 0.2 convert_bitcast_fusion.1
  32.7 0.5 copy.370
  33.2 0.5 copy.369
  33.6 1.3 fusion.49
  35.0 2.8 %fusion.10 = (bf16[512,8,64]{2,0,1:T(8,128)(2,1)S(1)}, bf16[512,8,64]{2,0,1:T(8,128)(2,1)S(1)}, f32[512,8,64]{2,0,1:T(8,128)S(1)}, f32[512,8,64]{2,0,1:T(8,128)}) fusion(f32[1,512,8,64]{3,2,1,0:T(8,128)S(1)} %get-tuple-element.67, f32[1,512,8,64]{3,2,1,0:T(8,128)S(1)} %get-tuple-element.66, f32[512,64]{1,0:T(8,128)S(1)} %get-tuple-element.93, ...), kind=kLoop, calls=%fused_computation.27 | loop fusion | flops 3670016 | bytes 7602176 | tf_op jit(solution)/shard_map/concatenate | solution.py:19
  37.8 2.4 %convolution_convert_fusion.2 = bf16[513,1024]{1,0:T(8,128)(2,1)S(1)} fusion(bf16[513,2048]{1,0:T(8,128)(2,1)S(1)} %copy-done.7, bf16[2048,1024]{1,0:T(8,128)(2,1)S(1)} %copy-done.6), kind=kOutput, calls=%fused_computation.22 | convolution fusion | flops 2152203264 | bytes 7346176 | tf_op jit(solution)/shard_map/dot_general | solution.py:57
  40.3 2.6 %convolution_bitcast_fusion = f32[1,1,8,128,128]{4,3,2,1,0:T(8,128)S(1)} fusion(f32[512,8]{0,1:T(8,128)S(1)} %get-tuple-element.98, bf16[512,8,64]{2,0,1:T(8,128)(2,1)S(1)} %get-tuple-element.63, bf16[512,8,64]{2,0,1:T(8,128)(2,1)S(1)} %get-tuple-element.62, bf16[513,1024]{1,0:T(8,128)(2,1)S(1)} %convolution_convert_fusion.2), kind=kOutput, calls=%fused_computation.23 | convolution fusion | flops 137363456 | bytes 3686400 | tf_op jit(solution)/shard_map/smhd,smhe->shde/dot_general | solution.py:73
  42.9 1.1 copy.333
  44.1 6.8 %all-to-all-start = ((f32[1,1,8,128,128]{4,2,1,0,3:T(8,128)}), f32[1,1,8,128,128]{4,2,1,0,3:T(8,128)S(1)}, u32[]{:S(2)}, u32[]{:S(2)}) async-start(f32[1,1,8,128,128]{4,2,1,0,3:T(8,128)} %copy.333), calls=%async_computation | async-start | bytes 1048576 | tf_op jit(solution)/shard_map/all_to_all | solution.py:76
  50.9 0.1 fusion.40
  50.9 0.1 fusion.35
  51.0 0.1 dynamic-slice_bitcast_fusion
  51.1 0.2 multiply_reduce_fusion.2
  51.3 3.2 %fusion.7 = bf16[512,8,128]{2,0,1:T(8,128)(2,1)} fusion(f32[512,8,64]{2,0,1:T(8,128)S(1)} %get-tuple-element.70, f32[512,8,64]{2,0,1:T(8,128)} %get-tuple-element.71), kind=kLoop, calls=%fused_computation.8 | loop fusion | flops 1572864 | bytes 3145728 | tf_op jit(solution)/shard_map/convert_element_type | solution.py:68
  54.5 0.7 slice_convert_fusion
  55.2 7.4 %fusion = f32[8,128,512]{2,1,0:T(8,128)} fusion(f32[8]{0:T(128)S(1)} %get-tuple-element.97, f32[512,512]{1,0:T(8,128)} %fusion.15, pred[512,512]{1,0:T(8,128)(4,1)S(1)} %fusion.16, bf16[512,8,128]{2,0,1:T(8,128)(2,1)} %fusion.7, bf16[512,8,64]{2,0,1:T(8,128)(2,1)} %copy-done.2, bf16[512,8,64]{2,0,1:T(8,128)(2,1)} %copy-done.1, bf16[513,1024]{1,0:T(8,128)(2,1)} %copy-done.4), kind=kOutput, calls=%fused_computation.1 | convolution fusion | flops 1084227584 | bytes 7602208 | tf_op jit(solution)/shard_map/shnm,smhe->snhe/dot_general | solution.py:100
  62.6 3.8 %all-to-all-done = f32[1,1,8,128,128]{4,2,1,0,3:T(8,128)S(1)} async-done(((f32[1,1,8,128,128]{4,2,1,0,3:T(8,128)}), f32[1,1,8,128,128]{4,2,1,0,3:T(8,128)S(1)}, u32[]{:S(2)}, u32[]{:S(2)}) %all-to-all-start) | async-done | bytes 524320 | tf_op jit(solution)/shard_map/all_to_all | solution.py:76
  66.3 0.7 fusion.19
  67.1 0.1 fusion.38
  67.2 39.2 %psum.7 = f32[1,8,128]{2,1,0:T(8,128)S(1)} all-reduce(f32[1,8,128]{2,1,0:T(8,128)S(1)} %bitcast.159), channel_id=1, replica_groups=mesh['sp'=16,'tp'=2] {'sp'}, use_global_device_ids=true, to_apply=%region_2.3 | all-reduce | flops 1024 | bytes 8192 | tf_op jit(solution)/shard_map/psum | solution.py:131
  106.4 0.2 fusion.48
  106.6 0.9 fusion.9
  107.5 0.5 fusion.51
  108.1 0.6 constant_dynamic-update-slice_fusion.15
  108.7 0.6 constant_dynamic-update-slice_fusion.14
  109.3 0.6 constant_dynamic-update-slice_fusion.13
  109.9 0.6 constant_dynamic-update-slice_fusion.12
  110.5 0.6 constant_dynamic-update-slice_fusion.11
  111.1 0.6 constant_dynamic-update-slice_fusion.10
  111.7 0.6 constant_dynamic-update-slice_fusion.9
  112.3 0.6 constant_dynamic-update-slice_fusion.8
  112.9 0.6 constant_dynamic-update-slice_fusion.7
  113.5 0.6 constant_dynamic-update-slice_fusion.6
  114.1 0.6 constant_dynamic-update-slice_fusion.5
  114.7 0.6 constant_dynamic-update-slice_fusion.4
  115.3 0.6 constant_dynamic-update-slice_fusion.3
  115.9 0.6 constant_dynamic-update-slice_fusion.2
  116.5 0.6 constant_dynamic-update-slice_fusion.1
  117.1 0.6 constant_dynamic-update-slice_fusion
  117.7 3.5 %all-to-all-start.1 = ((bf16[16,1,1,8,8,128]{5,4,3,2,1,0:T(8,128)(2,1)}), bf16[16,1,1,8,8,128]{5,4,3,2,1,0:T(8,128)(2,1)S(1)}, u32[]{:S(2)}, u32[]{:S(2)}) async-start(bf16[16,1,1,8,8,128]{5,4,3,2,1,0:T(8,128)(2,1)} %constant_dynamic-update-slice_fusion), calls=%async_computation.1 | async-start | bytes 524288 | tf_op jit(solution)/shard_map/all_to_all | solution.py:88
  121.3 0.2 multiply_reduce_fusion.1
  121.5 0.1 fusion.42
  121.5 0.6 copy.429
  122.1 0.6 convert_bitcast_fusion.2
  122.7 7.0 %all-to-all-done.1 = bf16[16,1,1,8,8,128]{5,4,3,2,1,0:T(8,128)(2,1)S(1)} async-done(((bf16[16,1,1,8,8,128]{5,4,3,2,1,0:T(8,128)(2,1)}), bf16[16,1,1,8,8,128]{5,4,3,2,1,0:T(8,128)(2,1)S(1)}, u32[]{:S(2)}, u32[]{:S(2)}) %all-to-all-start.1) | async-done | bytes 262176 | tf_op jit(solution)/shard_map/all_to_all | solution.py:88
  129.7 2.1 %fusion.52 = (f32[512,8]{0,1:T(8,128)S(1)}, f32[1,512,8,128]{1,3,2,0:T(8,128)S(1)}) fusion(f32[512,8]{0,1:T(8,128)S(1)} %get-tuple-element.99, bf16[512,8,128]{2,0,1:T(8,128)(2,1)S(1)} %copy-done, f32[8,128,512]{2,1,0:T(8,128)} %fusion, bf16[16,1,1,8,8,128]{5,4,3,2,1,0:T(8,128)(2,1)S(1)} %all-to-all-done.1), kind=kOutput, calls=%fused_computation.123 | convolution fusion | flops 135786496 | bytes 5537792 | tf_op jit(solution)/shard_map/snhd,shde->snhe/dot_general | solution.py:104
  131.9 0.3 multiply_reduce_fusion
  132.2 0.4 multiply_convert_fusion.2
  132.5 1.3 copy.338
  (30 shorter events, 0.1 us)
Async XLA Ops:
  7.2 15.9 %all-gather.2.cloned.1.call-start = ((), (), s32[]{:S(2)}) async-start(), calls=%async_computation.2 | async-start | bytes 3194880 | tf_op jit(solution)/shard_map/all_gather | solution.py:55
  7.2 3.9 %copy-start.8 = (f32[8]{0:T(128)S(1)}, f32[8]{0:T(128)}, u32[]{:S(2)}) copy-start(f32[8]{0:T(128)} %param.12) | copy-start | bytes 100
  23.0 5.6 %copy-start.5 = (bf16[2048,1024]{1,0:T(8,128)(2,1)S(1)}, bf16[2048,1024]{1,0:T(8,128)(2,1)}, u32[]{:S(2)}) copy-start(bf16[2048,1024]{1,0:T(8,128)(2,1)} %param.9) | copy-start | bytes 12582916
  28.4 1.6 %copy-start.7 = (bf16[513,2048]{1,0:T(8,128)(2,1)S(1)}, bf16[513,2048]{1,0:T(8,128)(2,1)}, u32[]{:S(2)}) copy-start(bf16[513,2048]{1,0:T(8,128)(2,1)} %all-gather.2.cloned.1.call-done) | copy-start | bytes 6303748
  35.0 2.8 %copy-start.6 = (bf16[2048,1024]{1,0:T(8,128)(2,1)S(1)}, bf16[2048,1024]{1,0:T(8,128)(2,1)}, u32[]{:S(2)}) copy-start(bf16[2048,1024]{1,0:T(8,128)(2,1)} %param.11) | copy-start | bytes 12582916
  37.8 2.4 %copy-start.1 = (bf16[512,8,64]{2,0,1:T(8,128)(2,1)}, bf16[512,8,64]{2,0,1:T(8,128)(2,1)S(1)}, u32[]{:S(2)}) copy-start(bf16[512,8,64]{2,0,1:T(8,128)(2,1)S(1)} %get-tuple-element.62) | copy-start | bytes 1572868
  37.8 2.4 %copy-start.2 = (bf16[512,8,64]{2,0,1:T(8,128)(2,1)}, bf16[512,8,64]{2,0,1:T(8,128)(2,1)S(1)}, u32[]{:S(2)}) copy-start(bf16[512,8,64]{2,0,1:T(8,128)(2,1)S(1)} %get-tuple-element.63) | copy-start | bytes 1572868
  40.2 2.7 %copy-start.4 = (bf16[513,1024]{1,0:T(8,128)(2,1)}, bf16[513,1024]{1,0:T(8,128)(2,1)S(1)}, u32[]{:S(2)}) copy-start(bf16[513,1024]{1,0:T(8,128)(2,1)S(1)} %convolution_convert_fusion.2) | copy-start | bytes 3151876
  44.1 22.3 %all-to-all-start = ((f32[1,1,8,128,128]{4,2,1,0,3:T(8,128)}), f32[1,1,8,128,128]{4,2,1,0,3:T(8,128)S(1)}, u32[]{:S(2)}, u32[]{:S(2)}) async-start(f32[1,1,8,128,128]{4,2,1,0,3:T(8,128)} %copy.333), calls=%async_computation | async-start | bytes 1048576 | tf_op jit(solution)/shard_map/all_to_all | solution.py:76
  62.6 58.9 %copy-start.3 = (f32[1024]{0:T(1024)S(1)}, f32[1024]{0:T(1024)}, u32[]{:S(2)}) copy-start(f32[1024]{0:T(1024)} %param.13) | copy-start | bytes 12292
  62.6 67.1 %copy-start = (bf16[512,8,128]{2,0,1:T(8,128)(2,1)S(1)}, bf16[512,8,128]{2,0,1:T(8,128)(2,1)}, u32[]{:S(2)}) copy-start(bf16[512,8,128]{2,0,1:T(8,128)(2,1)} %fusion.7) | copy-start | bytes 3145732
  117.7 12.0 %all-to-all-start.1 = ((bf16[16,1,1,8,8,128]{5,4,3,2,1,0:T(8,128)(2,1)}), bf16[16,1,1,8,8,128]{5,4,3,2,1,0:T(8,128)(2,1)S(1)}, u32[]{:S(2)}, u32[]{:S(2)}) async-start(bf16[16,1,1,8,8,128]{5,4,3,2,1,0:T(8,128)(2,1)} %constant_dynamic-update-slice_fusion), calls=%async_computation.1 | async-start | bytes 524288 | tf_op jit(solution)/shard_map/all_to_all | solution.py:88
Sparse Core Ops, SparseCore 0:
  9.7 13.3 all-gather.1
